TPU v7x, 512 devices: a whole 4x4x16 slice. The times are simulated.
512 devices in a mesh: fs: 16 (over y, x), tp: 32 (over z, core).
Axes of the slice: x: 4, y: 4, z: 16, core: 2. Of those that a mesh axis runs over, the one named last changes fastest.
Arguments:
- saved_inputs: bfloat16 [10752, 4096], P('fs', 'tp'), may hold values from -6 to 6
- proj_cotangent: bfloat16 [10752, 4096], P('fs', 'tp'), may hold values from -0.057861328 to 0.057861328
- saved_hidden: bfloat16 [10752, 4096], P('fs', 'tp'), may hold values from -6 to 6
- out_cotangent: bfloat16 [10752, 4096], P('fs', 'tp'), may hold values from -0.057861328 to 0.057861328
- factors: bfloat16 [2, 4096, 128], replicated, may hold values from -0.46875 to 0.46875
- w_proj: float32 [4096, 4096], P('fs', 'tp'), may hold values from -0.09375 to 0.09375
- w_out: float32 [4096, 4096], P('tp', 'fs'), may hold values from -0.09375 to 0.09375
- moment_first: float32 [2, 128, 4096], P(None, None, 'tp'), may hold values from -1.8 to 1.8
- moment_second: float32 [2, 128, 4096], P(None, None, 'tp'), may hold values from 0.05 to 1
Outputs:
- proj_next: float32 [4096, 4096], P('fs', 'tp')
- out_next: float32 [4096, 4096], P('tp', 'fs')
- proj_copy: bfloat16 [4096, 4096], P(None, 'tp')
- out_copy: bfloat16 [4096, 4096], P('tp')
- first_next: float32 [2, 128, 4096], P(None, None, 'tp')
- second_next: float32 [2, 128, 4096], P(None, None, 'tp')
All inputs are finite; a program needn't handle non-finite values.
Results may differ from a plain program's by a relative error of at most 0.001.
Values may be sent and summed in bfloat16 or wider, within the bound.
No kernel may reach another device: no remote copies, remote signals or barrier semaphores. Data moves between devices by JAX's collectives and lax.ppermute only.
A program may use at most 64 MiB of HBM per device.

v0:
```python
import jax
import jax.numpy as jnp
from jax import lax
from jax.sharding import Mesh
from jax.sharding import PartitionSpec as P

FS = ("fs_0", "fs_1")
TP = ("tp_0", "tp_1")
beta_first = 0.9
beta_second = 0.95
learn_rate = 0.02
epsilon = 1e-06


def split_up(x, dim, count):
    before, after = (x.shape[:dim], x.shape[dim + 1 :])
    return jnp.moveaxis(x.reshape(*before, count, -1, *after), dim, 0)


def sum_at_owner(x, axis, dim):
    count = lax.axis_size(axis)
    blocks = lax.all_to_all(split_up(x, dim, count), axis, 0, 0, tiled=True)
    return jnp.sum(blocks, axis=0)


def rows_for(lines, count):
    spare = -lines.shape[0] % count
    if not spare:
        return lines
    return jnp.concatenate([lines, jnp.zeros((spare, *lines.shape[1:]), lines.dtype)])


def sent_to_all(x, axis):
    count = lax.axis_size(axis)
    return lax.all_to_all(jnp.broadcast_to(x[None], (count, *x.shape)), axis, 0, 0, tiled=True)


def in_order(blocks, dim):
    blocks = jnp.moveaxis(blocks, 0, dim)
    dims = blocks.shape
    return blocks.reshape(*dims[:dim], dims[dim] * dims[dim + 1], *dims[dim + 2 :])


def gather_directly(x, axis, dim):
    blocks = sent_to_all(x, axis)
    return in_order(blocks, dim)


def sum_by_parts(x, axes):
    own = sum_at_owner(rows_for(x, lax.axis_size(axes)), axes, 0)
    whole = gather_directly(own, axes, 0)
    return whole[: len(x)].reshape(x.shape)


def packed_total(arrays, axis):
    ends = [0]
    for a in arrays:
        ends.append(ends[-1] + a.size)
    total = sum_by_parts(jnp.concatenate([a.ravel() for a in arrays]), axis)
    return tuple((total[b:e].reshape(a.shape) for a, b, e in zip(arrays, ends, ends[1:])))


def total_of(x, axes):
    lines = x.reshape(-1, x.shape[-1])
    own = sum_at_owner(rows_for(lines, lax.axis_size(axes)), axes, 0)
    whole = gather_directly(own, axes, 0)
    return whole[: len(lines)].reshape(x.shape)


def of_everyone(x, axis):
    return sent_to_all(x, axis).sum(axis=0)


def one_axis_at_a_time(x, axes):
    far, near = axes
    nearer = of_everyone(x, near)
    return of_everyone(nearer, far)


def gather_turned(arrays, axis, dims):
    turned = [jnp.moveaxis(a, dim, 0) for a, dim in zip(arrays, dims)]
    widths = [t[0].size for t in turned]
    both = jnp.concatenate([t.reshape(-1, w) for t, w in zip(turned, widths)], axis=1)
    result = lax.all_gather(both, axis, axis=0, tiled=True)
    blocks = jnp.split(result, [sum(widths[:k]) for k in range(1, len(widths))], axis=1)
    return tuple(
        (
            jnp.moveaxis(b.reshape(-1, *t.shape[1:]), 0, dim)
            for b, t, dim in zip(blocks, turned, dims)
        )
    )


def over_tokens(left_rows, right_rows, precise):
    return lax.dot_general(
        left_rows,
        right_rows,
        (((0,), (0,)), ((), ())),
        preferred_element_type=jnp.float32,
        precision=precise,
    )


def body(
    saved_inputs,
    proj_cotangent,
    saved_hidden,
    out_cotangent,
    factors,
    w_proj,
    w_out,
    moment_first,
    moment_second,
):
    highest = lax.Precision.HIGHEST
    fs_count = lax.axis_size(FS)
    tp_count = lax.axis_size(TP)
    d_model = factors.shape[1]
    hidden_width = proj_cotangent.shape[1]
    fs_rows = d_model // fs_count
    tp_feats = saved_inputs.shape[1]
    own_rows = lax.dynamic_slice_in_dim(factors, lax.axis_index(FS) * fs_rows, fs_rows, 1).astype(
        jnp.float32
    )
    own_feats = lax.dynamic_slice_in_dim(factors, lax.axis_index(TP) * tp_feats, tp_feats, 1)
    proj_rows = jnp.dot(saved_inputs, own_feats[0], preferred_element_type=jnp.float32)
    out_rows = jnp.dot(out_cotangent, own_feats[1], preferred_element_type=jnp.float32)
    proj_rows, out_rows = packed_total((proj_rows, out_rows), TP)
    partial_sums = jnp.stack(
        [
            over_tokens(proj_rows, proj_cotangent.astype(jnp.float32), highest),
            over_tokens(out_rows, saved_hidden.astype(jnp.float32), highest),
        ]
    )
    small_grads = total_of(partial_sums, FS)
    first_next = beta_first * moment_first + (1.0 - beta_first) * small_grads
    second_next = beta_second * moment_second + (1.0 - beta_second) * small_grads * small_grads
    direction = first_next / (jnp.sqrt(second_next) + epsilon)
    update_full = jnp.einsum("kdr,kre->kde", own_rows, direction, precision=highest)
    squares = one_axis_at_a_time(
        jnp.sum(update_full * update_full, axis=(1, 2)), (("fs_0", "fs_1"), ("tp_0", "tp_1"))
    )
    norm_scale = lax.rsqrt(squares / (d_model * hidden_width * tp_count) + epsilon)
    stepped = update_full * norm_scale[:, None, None]
    proj_next = w_proj - learn_rate * stepped[0]
    out_next = w_out - learn_rate * stepped[1].T
    proj_copy, out_copy = gather_turned(
        (proj_next.astype(jnp.bfloat16), out_next.astype(jnp.bfloat16)), FS, (0, 1)
    )
    return (proj_next, out_next, proj_copy, out_copy, first_next, second_next)


def solution(mesh):
    torus = Mesh(mesh.devices.reshape(4, 4, 16, 2), ("fs_0", "fs_1", "tp_0", "tp_1"))
    return jax.shard_map(
        body,
        mesh=torus,
        in_specs=(
            P(FS, TP),
            P(FS, TP),
            P(FS, TP),
            P(FS, TP),
            P(),
            P(FS, TP),
            P(TP, FS),
            P(None, None, TP),
            P(None, None, TP),
        ),
        out_specs=(
            P(FS, TP),
            P(TP, FS),
            P(None, TP),
            P(TP, None),
            P(None, None, TP),
            P(None, None, TP),
        ),
        check_vma=False,
    )
```

profile of v0, /device:TPU:2, one launch (start us, length us, event | category | flops | bytes accessed | tf_op | source)
XLA Modules:
  0.0 230.2 jit_solution(13127133460400732446)
XLA Ops:
  7.2 0.0 copy-start
  7.2 1.6 copy-done
  8.8 1.1 convolution_bitcast_fusion
  9.9 0.1 concatenate.12
  9.9 1.1 convolution_bitcast_fusion.1
  11.1 0.1 concatenate.11
  11.2 0.5 all_to_all.24
  11.7 56.0 %all_to_all.37 = f32[32,1,5376]{2,1,0:T(1,128)S(1)} all-to-all(f32[32,1,5376]{2,1,0:T(1,128)S(1)} %all_to_all.24), channel_id=1, replica_groups=mesh['fs_0'=4,'fs_1'=4,'tp_0'=16,'tp_1'=2] {'tp_0','tp_1'}, dimensions={0} | all-to-all | bytes 1376256 | tf_op jit(solution)/shard_map/all_to_all | solution.py:22
  67.7 0.0 copy-start.1
  67.7 0.4 reduce_sum.45
  68.1 0.0 copy-start.2
  68.1 0.4 broadcast_in_dim.8
  68.5 44.0 %all_to_all.38 = f32[32,1,5376]{2,1,0:T(1,128)S(1)} all-to-all(f32[32,1,5376]{2,1,0:T(1,128)S(1)} %broadcast_in_dim.8), channel_id=1, replica_groups=mesh['fs_0'=4,'fs_1'=4,'tp_0'=16,'tp_1'=2] {'tp_0','tp_1'}, dimensions={0} | all-to-all | bytes 1376256 | tf_op jit(solution)/shard_map/all_to_all | solution.py:35
  112.5 0.1 fusion.19
  112.6 0.0 copy-start.8
  112.6 0.0 copy-done.1
  112.6 0.5 convolution_bitcast_fusion.3
  113.1 0.0 copy-done.2
  113.1 0.0 copy-start.5
  113.1 0.5 convolution_bitcast_fusion.2
  113.7 13.9 %all_to_all.39 = f32[16,16,128]{2,1,0:T(8,128)S(1)} all-to-all(f32[16,16,128]{2,1,0:T(8,128)S(1)} %bitcast.48), channel_id=1, replica_groups=mesh['fs_0'=4,'fs_1'=4,'tp_0'=16,'tp_1'=2] {'fs_0','fs_1'}, dimensions={0} | all-to-all | bytes 262144 | tf_op jit(solution)/shard_map/all_to_all | solution.py:22
  127.6 0.7 broadcast_in_dim.9
  128.3 4.8 %all-to-all-start.3 = ((f32[16,16,128]{2,1,0:T(8,128)}), f32[16,16,128]{2,1,0:T(8,128)S(1)}, u32[]{:S(2)}, u32[]{:S(2)}) async-start(f32[16,16,128]{2,1,0:T(8,128)} %broadcast_in_dim.9), calls=%async_computation.3 | async-start | bytes 262144 | tf_op jit(solution)/shard_map/all_to_all | solution.py:35
  133.0 6.7 %all-to-all-done.3 = f32[16,16,128]{2,1,0:T(8,128)S(1)} async-done(((f32[16,16,128]{2,1,0:T(8,128)}), f32[16,16,128]{2,1,0:T(8,128)S(1)}, u32[]{:S(2)}, u32[]{:S(2)}) %all-to-all-start.3) | async-done | bytes 131104 | tf_op jit(solution)/shard_map/all_to_all | solution.py:35
  139.8 0.0 copy-done.3
  139.8 0.0 copy-done.4
  139.8 0.0 copy-start.6
  139.8 0.0 copy-start.7
  139.8 0.4 multiply_reduce_fusion
  140.3 15.4 %all_to_all.40 = f32[32,1,2]{2,1,0:T(1,128)S(1)} all-to-all(f32[32,1,2]{2,1,0:T(1,128)S(1)} %broadcast_in_dim.10), channel_id=1, replica_groups=mesh['fs_0'=4,'fs_1'=4,'tp_0'=16,'tp_1'=2] {'tp_0','tp_1'}, dimensions={0} | all-to-all | bytes 512 | tf_op jit(solution)/shard_map/all_to_all | solution.py:35
  155.7 0.1 reduce_sum.48
  155.7 0.6 broadcast_in_dim.11
  156.4 4.7 %all-to-all-start.5 = ((f32[16,1,2]{2,1,0:T(1,128)}), f32[16,1,2]{2,1,0:T(1,128)S(1)}, u32[]{:S(2)}, u32[]{:S(2)}) async-start(f32[16,1,2]{2,1,0:T(1,128)} %broadcast_in_dim.11), calls=%async_computation.5 | async-start | bytes 16384 | tf_op jit(solution)/shard_map/all_to_all | solution.py:35
  161.1 0.0 all-gather.2.cloned.1.call-start
  161.1 0.0 copy-done.8
  161.1 0.1 copy.30
  161.2 6.1 %all-to-all-done.5 = f32[16,1,2]{2,1,0:T(1,128)S(1)} async-done(((f32[16,1,2]{2,1,0:T(1,128)}), f32[16,1,2]{2,1,0:T(1,128)S(1)}, u32[]{:S(2)}, u32[]{:S(2)}) %all-to-all-start.5) | async-done | bytes 160 | tf_op jit(solution)/shard_map/all_to_all | solution.py:35
  167.3 0.1 broadcast_multiply_fusion
  167.4 0.0 copy-done.5
  167.5 0.7 convert_bitcast_fusion
  168.1 0.7 pad_maximum_fusion.2
  168.8 0.0 all-gather.2.cloned.1.call-update
  168.8 0.8 copy.31
  169.6 49.8 %all-gather.2.cloned.1.call-done = bf16[4096,256]{0,1:T(8,128)(2,1)} async-done(((bf16[256,256]{0,1:T(8,128)(2,1)}), bf16[4096,256]{0,1:T(8,128)(2,1)}) %all-gather.2.cloned.1.call-update) | async-done | bytes 2097168 | tf_op jit(solution)/shard_map/all_gather | solution.py:84
  219.3 2.7 %slice_bitcast_fusion = (bf16[128,4096]{1,0:T(8,128)(2,1)}, bf16[4096,128]{0,1:T(8,128)(2,1)S(1)}) fusion(bf16[4096,256]{0,1:T(8,128)(2,1)} %all-gather.2.cloned.1.call-done), kind=kLoop, calls=%fused_computation.4 | loop fusion | bytes 4194304 | tf_op jit(solution)/shard_map/transpose | solution.py:88
  222.0 0.0 copy-done.6
  222.0 0.0 copy-done.7
  222.0 1.3 copy.32
  (10 shorter events, 0.2 us)
Async XLA Ops:
  7.2 1.6 copy-start
  67.7 44.9 %copy-start.1 = (bf16[672,128]{1,0:T(8,128)(2,1)S(1)}, bf16[672,128]{1,0:T(8,128)(2,1)}, u32[]{:S(2)}) copy-start(bf16[672,128]{1,0:T(8,128)(2,1)} %param.10) | copy-start | bytes 516100
  68.1 45.0 %copy-start.2 = (bf16[672,128]{1,0:T(8,128)(2,1)S(1)}, bf16[672,128]{1,0:T(8,128)(2,1)}, u32[]{:S(2)}) copy-start(bf16[672,128]{1,0:T(8,128)(2,1)} %param.11) | copy-start | bytes 516100
  112.5 27.2 %copy-start.3 = (f32[2,128,128]{2,1,0:T(8,128)S(1)}, f32[2,128,128]{2,1,0:T(8,128)}, u32[]{:S(2)}) copy-start(f32[2,128,128]{2,1,0:T(8,128)} %param.17) | copy-start | bytes 393220
  112.5 27.2 %copy-start.4 = (f32[2,128,128]{2,1,0:T(8,128)S(1)}, f32[2,128,128]{2,1,0:T(8,128)}, u32[]{:S(2)}) copy-start(f32[2,128,128]{2,1,0:T(8,128)} %param.16) | copy-start | bytes 393220
  112.6 48.5 %copy-start.8 = (f32[256,128]{1,0:T(8,128)S(1)}, f32[256,128]{1,0:T(8,128)}, u32[]{:S(2)}) copy-start(f32[256,128]{1,0:T(8,128)} %param.14) | copy-start | bytes 393220
  113.1 54.3 %copy-start.5 = (f32[128,256]{1,0:T(8,128)S(1)}, f32[128,256]{1,0:T(8,128)}, u32[]{:S(2)}) copy-start(f32[128,256]{1,0:T(8,128)} %param.15) | copy-start | bytes 393220
  128.3 11.5 %all-to-all-start.3 = ((f32[16,16,128]{2,1,0:T(8,128)}), f32[16,16,128]{2,1,0:T(8,128)S(1)}, u32[]{:S(2)}, u32[]{:S(2)}) async-start(f32[16,16,128]{2,1,0:T(8,128)} %broadcast_in_dim.9), calls=%async_computation.3 | async-start | bytes 262144 | tf_op jit(solution)/shard_map/all_to_all | solution.py:35
  139.8 82.2 %copy-start.6 = (f32[2,128,128]{2,1,0:T(8,128)}, f32[2,128,128]{2,1,0:T(8,128)S(1)}, u32[]{:S(2)}) copy-start(f32[2,128,128]{2,1,0:T(8,128)S(1)} %get-tuple-element.38) | copy-start | bytes 393220
  139.8 82.2 %copy-start.7 = (f32[2,128,128]{2,1,0:T(8,128)}, f32[2,128,128]{2,1,0:T(8,128)S(1)}, u32[]{:S(2)}) copy-start(f32[2,128,128]{2,1,0:T(8,128)S(1)} %get-tuple-element.39) | copy-start | bytes 393220
  156.4 10.9 %all-to-all-start.5 = ((f32[16,1,2]{2,1,0:T(1,128)}), f32[16,1,2]{2,1,0:T(1,128)S(1)}, u32[]{:S(2)}, u32[]{:S(2)}) async-start(f32[16,1,2]{2,1,0:T(1,128)} %broadcast_in_dim.11), calls=%async_computation.5 | async-start | bytes 16384 | tf_op jit(solution)/shard_map/all_to_all | solution.py:35
  161.1 58.3 %all-gather.2.cloned.1.call-start = ((), (), s32[]{:S(2)}) async-start(), calls=%async_computation.6 | async-start | bytes 2228224 | tf_op jit(solution)/shard_map/all_gather | solution.py:84
Sparse Core Ops, SparseCore 0:
  168.9 50.3 all-gather.1
where the time goes:
time: 231 us; the launch traced here: 230 us
  blocking collectives  129 us (56%)
  waiting for transfers between devices  62.5 us (27%)
  between operations  14.2 us (6%)
  starting transfers between devices  9.51 us (4%)
  local copies, waits for them, and re-layouts  8.78 us (4%)
  matrix products  3.67 us (2%)
    all_to_all x2, blocking collectives, sum_at_owner(): blocks = lax.all_to_all(split_up(x, dim, count), axis, 0, 0, tiled=True)  69.9 us
    all_to_all x2, blocking collectives, sent_to_all(): lax.all_to_all(jnp.broadcast_to(x[None], (count, *x.shape)), axis, 0, 0,...  59.4 us
    all_gather x1, waiting for transfers between devices, gather_turned(): result = lax.all_gather(both, axis, axis=0, tiled=True)  49.8 us
    all_to_all x2, waiting for transfers between devices, sent_to_all(): lax.all_to_all(jnp.broadcast_to(x[None], (count, *x.shape)), axis, 0, 0,...  12.8 us
    all_to_all x2, starting transfers between devices, sent_to_all(): lax.all_to_all(jnp.broadcast_to(x[None], (count, *x.shape)), axis, 0, 0,...  9.48 us
  transfers between devices with their start and end apart: 3, of which 3 were waited for; matrix products, arithmetic and copies ran while one was open for 0% of the time, Pallas kernels for 0%

commit v1 on v0

--- a/solution.py
+++ b/solution.py
@@ -81,7 +81,14 @@
     turned = [jnp.moveaxis(a, dim, 0) for a, dim in zip(arrays, dims)]
     widths = [t[0].size for t in turned]
     both = jnp.concatenate([t.reshape(-1, w) for t, w in zip(turned, widths)], axis=1)
-    result = lax.all_gather(both, axis, axis=0, tiled=True)
+
+    def limits_bring(row_data):
+        everything = jnp.stack([row_data for _ in range(lax.axis_size(axis))], axis=0)
+        earlier = lax.all_to_all(everything, axis, split_axis=0, concat_axis=0)
+        work_now = jnp.concatenate(earlier, axis=0)
+        return work_now
+
+    result = limits_bring(both)
     blocks = jnp.split(result, [sum(widths[:k]) for k in range(1, len(widths))], axis=1)
     return tuple(
         (

time: 231 us -> 205 us (0.89)
  the two profiles are of different devices: /device:TPU:2 before, /device:TPU:32 now
where the time goes in v1:
time: 205 us
  blocking collectives  129 us (63%)
  waiting for transfers between devices  44 us (21%)
  local copies, waits for them, and re-layouts  14.2 us (7%)
  starting transfers between devices  11.4 us (6%)
  matrix products  3.67 us (2%)
    all_to_all x2, blocking collectives, sum_at_owner(): blocks = lax.all_to_all(split_up(x, dim, count), axis, 0, 0, tiled=True)  69.2 us
    all_to_all x2, blocking collectives, sent_to_all(): lax.all_to_all(jnp.broadcast_to(x[None], (count, *x.shape)), axis, 0, 0,...  59.7 us
    all_to_all x1, waiting for transfers between devices, limits_bring(): earlier = lax.all_to_all(everything, axis, split_axis=0, concat_axis=0)  28.8 us
    all_to_all x2, waiting for transfers between devices, sent_to_all(): lax.all_to_all(jnp.broadcast_to(x[None], (count, *x.shape)), axis, 0, 0,...  15.3 us
    all_to_all x2, starting transfers between devices, sent_to_all(): lax.all_to_all(jnp.broadcast_to(x[None], (count, *x.shape)), axis, 0, 0,...  6.98 us
    all_to_all x1, starting transfers between devices, limits_bring(): earlier = lax.all_to_all(everything, axis, split_axis=0, concat_axis=0)  4.44 us
  transfers between devices with their start and end apart: 3, of which 3 were waited for; matrix products, arithmetic and copies ran while one was open for 0% of the time, Pallas kernels for 0%

profile of v1, /device:TPU:32, one launch (start us, length us, event | category | flops | bytes accessed | tf_op | source)
XLA Modules:
  0.0 204.5 jit_solution(13621514391069984315)
XLA Ops:
  0.6 0.0 copy-start
  0.7 1.6 copy-done
  2.2 1.1 convolution_bitcast_fusion
  3.3 0.1 concatenate.12
  3.4 1.1 convolution_bitcast_fusion.1
  4.5 0.1 concatenate.11
  4.7 0.5 all_to_all.27
  5.1 54.4 %all_to_all.42 = f32[32,1,5376]{2,1,0:T(1,128)S(1)} all-to-all(f32[32,1,5376]{2,1,0:T(1,128)S(1)} %all_to_all.27), channel_id=1, replica_groups=mesh['fs_0'=4,'fs_1'=4,'tp_0'=16,'tp_1'=2] {'tp_0','tp_1'}, dimensions={0} | all-to-all | bytes 1376256 | tf_op jit(solution)/shard_map/all_to_all | solution.py:22
  59.6 0.0 copy-start.1
  59.6 0.4 reduce_sum.45
  60.0 0.0 copy-start.2
  60.0 0.4 broadcast_in_dim.8
  60.3 43.6 %all_to_all.43 = f32[32,1,5376]{2,1,0:T(1,128)S(1)} all-to-all(f32[32,1,5376]{2,1,0:T(1,128)S(1)} %broadcast_in_dim.8), channel_id=1, replica_groups=mesh['fs_0'=4,'fs_1'=4,'tp_0'=16,'tp_1'=2] {'tp_0','tp_1'}, dimensions={0} | all-to-all | bytes 1376256 | tf_op jit(solution)/shard_map/all_to_all | solution.py:35
  103.9 0.1 fusion.19
  104.0 0.0 copy-start.8
  104.0 0.0 copy-done.1
  104.0 0.5 convolution_bitcast_fusion.3
  104.5 0.0 copy-done.2
  104.5 0.0 copy-start.5
  104.6 0.5 convolution_bitcast_fusion.2
  105.1 14.8 %all_to_all.44 = f32[16,16,128]{2,1,0:T(8,128)S(1)} all-to-all(f32[16,16,128]{2,1,0:T(8,128)S(1)} %bitcast.50), channel_id=1, replica_groups=mesh['fs_0'=4,'fs_1'=4,'tp_0'=16,'tp_1'=2] {'fs_0','fs_1'}, dimensions={0} | all-to-all | bytes 262144 | tf_op jit(solution)/shard_map/all_to_all | solution.py:22
  120.0 0.7 broadcast_in_dim.9
  120.6 3.5 %all-to-all-start.3 = ((f32[16,16,128]{2,1,0:T(8,128)}), f32[16,16,128]{2,1,0:T(8,128)S(1)}, u32[]{:S(2)}, u32[]{:S(2)}) async-start(f32[16,16,128]{2,1,0:T(8,128)} %broadcast_in_dim.9), calls=%async_computation.3 | async-start | bytes 262144 | tf_op jit(solution)/shard_map/all_to_all | solution.py:35
  124.2 7.9 %all-to-all-done.3 = f32[16,16,128]{2,1,0:T(8,128)S(1)} async-done(((f32[16,16,128]{2,1,0:T(8,128)}), f32[16,16,128]{2,1,0:T(8,128)S(1)}, u32[]{:S(2)}, u32[]{:S(2)}) %all-to-all-start.3) | async-done | bytes 131104 | tf_op jit(solution)/shard_map/all_to_all | solution.py:35
  132.1 0.0 copy-done.3
  132.1 0.0 copy-done.4
  132.1 0.0 copy-start.6
  132.2 0.0 copy-start.7
  132.2 0.4 multiply_reduce_fusion
  132.6 16.1 %all_to_all.45 = f32[32,1,2]{2,1,0:T(1,128)S(1)} all-to-all(f32[32,1,2]{2,1,0:T(1,128)S(1)} %broadcast_in_dim.10), channel_id=1, replica_groups=mesh['fs_0'=4,'fs_1'=4,'tp_0'=16,'tp_1'=2] {'tp_0','tp_1'}, dimensions={0} | all-to-all | bytes 512 | tf_op jit(solution)/shard_map/all_to_all | solution.py:35
  148.8 0.1 reduce_sum.48
  148.8 0.6 broadcast_in_dim.11
  149.4 3.5 %all-to-all-start.5 = ((f32[16,1,2]{2,1,0:T(1,128)}), f32[16,1,2]{2,1,0:T(1,128)S(1)}, u32[]{:S(2)}, u32[]{:S(2)}) async-start(f32[16,1,2]{2,1,0:T(1,128)} %broadcast_in_dim.11), calls=%async_computation.5 | async-start | bytes 16384 | tf_op jit(solution)/shard_map/all_to_all | solution.py:35
  152.9 0.0 copy-done.8
  152.9 0.1 copy.36
  153.0 7.3 %all-to-all-done.5 = f32[16,1,2]{2,1,0:T(1,128)S(1)} async-done(((f32[16,1,2]{2,1,0:T(1,128)}), f32[16,1,2]{2,1,0:T(1,128)S(1)}, u32[]{:S(2)}, u32[]{:S(2)}) %all-to-all-start.5) | async-done | bytes 160 | tf_op jit(solution)/shard_map/all_to_all | solution.py:35
  160.4 0.1 broadcast_multiply_fusion
  160.5 0.0 copy-done.5
  160.5 0.7 convert_bitcast_fusion
  161.2 1.5 stack.11
  162.7 0.0 copy-done.6
  162.7 0.0 copy-done.7
  162.7 4.4 %all-to-all-start.6 = ((bf16[16,256,256]{1,2,0:T(8,128)(2,1)}), bf16[16,256,256]{1,2,0:T(8,128)(2,1)}, u32[]{:S(2)}, u32[]{:S(2)}) async-start(bf16[16,256,256]{1,2,0:T(8,128)(2,1)} %stack.11), calls=%async_computation.6 | async-start | bytes 4194304 | tf_op jit(solution)/shard_map/all_to_all | solution.py:87
  167.2 0.8 copy.38
  167.9 28.8 %all-to-all-done.6 = bf16[16,256,256]{1,2,0:T(8,128)(2,1)} async-done(((bf16[16,256,256]{1,2,0:T(8,128)(2,1)}), bf16[16,256,256]{1,2,0:T(8,128)(2,1)}, u32[]{:S(2)}, u32[]{:S(2)}) %all-to-all-start.6) | async-done | bytes 2097184 | tf_op jit(solution)/shard_map/all_to_all | solution.py:87
  196.7 3.9 %copy.37 = bf16[16,256,256]{2,1,0:T(8,128)(2,1)} copy(bf16[16,256,256]{1,2,0:T(8,128)(2,1)} %all-to-all-done.6) | data formatting | bytes 4194304 | tf_op jit(solution)/shard_map/all_to_all | solution.py:87
  200.6 2.6 %slice_bitcast_fusion = (bf16[128,4096]{0,1:T(8,128)(2,1)S(1)}, bf16[4096,128]{1,0:T(8,128)(2,1)}) fusion(bf16[4096,256]{1,0:T(8,128)(2,1)} %bitcast.46), kind=kLoop, calls=%fused_computation.4 | loop fusion | bytes 4194304 | tf_op jit(solution)/shard_map/transpose | solution.py:95
  203.2 1.3 copy.39
  (11 shorter events, 0.2 us)
Async XLA Ops:
  0.6 1.6 copy-start
  59.6 44.5 %copy-start.1 = (bf16[672,128]{1,0:T(8,128)(2,1)S(1)}, bf16[672,128]{1,0:T(8,128)(2,1)}, u32[]{:S(2)}) copy-start(bf16[672,128]{1,0:T(8,128)(2,1)} %param.10) | copy-start | bytes 516100
  60.0 44.6 %copy-start.2 = (bf16[672,128]{1,0:T(8,128)(2,1)S(1)}, bf16[672,128]{1,0:T(8,128)(2,1)}, u32[]{:S(2)}) copy-start(bf16[672,128]{1,0:T(8,128)(2,1)} %param.11) | copy-start | bytes 516100
  103.9 28.2 %copy-start.3 = (f32[2,128,128]{2,1,0:T(8,128)S(1)}, f32[2,128,128]{2,1,0:T(8,128)}, u32[]{:S(2)}) copy-start(f32[2,128,128]{2,1,0:T(8,128)} %param.17) | copy-start | bytes 393220
  103.9 28.2 %copy-start.4 = (f32[2,128,128]{2,1,0:T(8,128)S(1)}, f32[2,128,128]{2,1,0:T(8,128)}, u32[]{:S(2)}) copy-start(f32[2,128,128]{2,1,0:T(8,128)} %param.16) | copy-start | bytes 393220
  104.0 48.9 %copy-start.8 = (f32[256,128]{1,0:T(8,128)S(1)}, f32[256,128]{1,0:T(8,128)}, u32[]{:S(2)}) copy-start(f32[256,128]{1,0:T(8,128)} %param.14) | copy-start | bytes 393220
  104.5 56.0 %copy-start.5 = (f32[128,256]{1,0:T(8,128)S(1)}, f32[128,256]{1,0:T(8,128)}, u32[]{:S(2)}) copy-start(f32[128,256]{1,0:T(8,128)} %param.15) | copy-start | bytes 393220
  120.6 11.5 %all-to-all-start.3 = ((f32[16,16,128]{2,1,0:T(8,128)}), f32[16,16,128]{2,1,0:T(8,128)S(1)}, u32[]{:S(2)}, u32[]{:S(2)}) async-start(f32[16,16,128]{2,1,0:T(8,128)} %broadcast_in_dim.9), calls=%async_computation.3 | async-start | bytes 262144 | tf_op jit(solution)/shard_map/all_to_all | solution.py:35
  132.1 30.6 %copy-start.6 = (f32[2,128,128]{2,1,0:T(8,128)}, f32[2,128,128]{2,1,0:T(8,128)S(1)}, u32[]{:S(2)}) copy-start(f32[2,128,128]{2,1,0:T(8,128)S(1)} %get-tuple-element.44) | copy-start | bytes 393220
  132.2 30.6 %copy-start.7 = (f32[2,128,128]{2,1,0:T(8,128)}, f32[2,128,128]{2,1,0:T(8,128)S(1)}, u32[]{:S(2)}) copy-start(f32[2,128,128]{2,1,0:T(8,128)S(1)} %get-tuple-element.45) | copy-start | bytes 393220
  149.4 10.9 %all-to-all-start.5 = ((f32[16,1,2]{2,1,0:T(1,128)}), f32[16,1,2]{2,1,0:T(1,128)S(1)}, u32[]{:S(2)}, u32[]{:S(2)}) async-start(f32[16,1,2]{2,1,0:T(1,128)} %broadcast_in_dim.11), calls=%async_computation.5 | async-start | bytes 16384 | tf_op jit(solution)/shard_map/all_to_all | solution.py:35
  162.7 34.0 %all-to-all-start.6 = ((bf16[16,256,256]{1,2,0:T(8,128)(2,1)}), bf16[16,256,256]{1,2,0:T(8,128)(2,1)}, u32[]{:S(2)}, u32[]{:S(2)}) async-start(bf16[16,256,256]{1,2,0:T(8,128)(2,1)} %stack.11), calls=%async_computation.6 | async-start | bytes 4194304 | tf_op jit(solution)/shard_map/all_to_all | solution.py:87
